TPU v7x, 32 devices: a whole 2x2x4 slice. The times are simulated.
32 devices in a mesh: sp: 8 (over z, x), dp: 4 (over y, core).
Axes of the slice: x: 2, y: 2, z: 4, core: 2. Of those that a mesh axis runs over, the one named last changes fastest.
Arguments:
- hidden_in: bfloat16 [4, 1024, 2048], P('dp', 'sp'), may hold values from -6 to 6
- in_weight: bfloat16 [2048, 512], P(('sp', 'dp')), may hold values from -0.125 to 0.125
- lam_real: float32 [32, 64], replicated, may hold values from -4 to 0, as said below
- lam_imag: float32 [32, 64], replicated, may hold values from 1 to 200
- log_step: float32 [32], replicated, may hold values from -4.61 to -2.3
- b_real: float32 [32, 64, 16], replicated, may hold values from -1 to 1
- b_imag: float32 [32, 64, 16], replicated, may hold values from -1 to 1
- c_real: float32 [32, 16, 64], replicated, may hold values from -0.3 to 0.3
- c_imag: float32 [32, 16, 64], replicated, may hold values from -0.3 to 0.3
- skip_weight: float32 [512], replicated, may hold values from -4 to 4
- lin_weight: bfloat16 [512, 2048], P(None, ('sp', 'dp')), may hold values from -0.25 to 0.25
- gate_weight: bfloat16 [512, 2048], P(None, ('sp', 'dp')), may hold values from -0.25 to 0.25
Outputs:
- mixed: bfloat16 [4, 1024, 2048], P('dp', 'sp')
Inputs may be any that keep to these rules, and one draw needn't show every extreme that they name: `lam_real`: negative in every entry.
All inputs are finite; a program needn't handle non-finite values.
Results may differ from a plain program's by a relative error of at most 0.0047.
The roundings to bfloat16 on the way count: a program that leaves them out, or rounds other values in their place, can miss the bound.
Values may be sent and summed in bfloat16 or wider, within the bound.
A program may use at most 64 MiB of HBM per device.

v0:
```python
import math

import jax
import jax.numpy as jnp
from jax import lax
from jax.sharding import PartitionSpec as P


def step_factors(lam_real, lam_imag, log_step, b_real, b_imag):
    step = jnp.exp(log_step)[:, None]
    xpart = lam_real * step
    wpart = lam_imag * step
    decay_re = jnp.exp(xpart) * jnp.cos(wpart)
    decay_im = jnp.exp(xpart) * jnp.sin(wpart)
    numer_re = jnp.expm1(xpart) * jnp.cos(wpart) - 2.0 * jnp.sin(0.5 * wpart) ** 2
    magnitude = lam_real * lam_real + lam_imag * lam_imag
    ratio_re = (numer_re * lam_real + decay_im * lam_imag) / magnitude
    ratio_im = (decay_im * lam_real - numer_re * lam_imag) / magnitude
    bbar_re = ratio_re[..., None] * b_real - ratio_im[..., None] * b_imag
    bbar_im = ratio_re[..., None] * b_imag + ratio_im[..., None] * b_real
    return (decay_re, decay_im, bbar_re, bbar_im)


def combine(left, right):
    lre, lim, lbre, lbim = left
    rre, rim, rbre, rbim = right
    return (
        rre * lre - rim * lim,
        rre * lim + rim * lre,
        rre * lbre - rim * lbim + rbre,
        rre * lbim + rim * lbre + rbim,
    )


def block_scan(piece, factors):
    decay_re, decay_im, bbar_re, bbar_im = factors
    highest = lax.Precision.HIGHEST
    block = piece.shape[0]
    groups_here, states = decay_re.shape
    lanes = groups_here * states
    source = piece.astype(jnp.float32)
    shaped = source.reshape(block, groups_here, source.shape[1] // groups_here)
    drive_re = jnp.einsum("tgh,gph->tgp", shaped, bbar_re, precision=highest).reshape(block, lanes)
    drive_im = jnp.einsum("tgh,gph->tgp", shaped, bbar_im, precision=highest).reshape(block, lanes)
    are = jnp.broadcast_to(decay_re.reshape(lanes), drive_re.shape)
    aim = jnp.broadcast_to(decay_im.reshape(lanes), drive_re.shape)
    return (source, lax.associative_scan(combine, (are, aim, drive_re, drive_im), axis=0))


def run_blocks(sequence, factors, out_re, out_im, direct, start):
    highest = lax.Precision.HIGHEST
    length, width = sequence.shape
    block = math.gcd(length, 512)
    blocks = sequence.reshape(length // block, block, width)
    groups_here, states = factors[0].shape

    def block_step(carry, piece):
        carry_re, carry_im = carry
        source, scanned = block_scan(piece, factors)
        cum_re, cum_im, local_re, local_im = scanned
        state_re = local_re + cum_re * carry_re - cum_im * carry_im
        state_im = local_im + cum_re * carry_im + cum_im * carry_re
        summed = jnp.einsum(
            "tgp,ghp->tgh", state_re.reshape(block, groups_here, states), out_re, precision=highest
        ) - jnp.einsum(
            "tgp,ghp->tgh", state_im.reshape(block, groups_here, states), out_im, precision=highest
        )
        result = jax.nn.gelu(summed.reshape(block, width) + direct * source)
        return ((state_re[-1], state_im[-1]), result.astype(jnp.bfloat16))

    _, results = lax.scan(block_step, start, blocks)
    return results.reshape(length, width)


def by_groups(sequence, lam_real, lam_imag, log_step, b_real, b_imag, c_real, c_imag, skip_weight):
    per_group = b_real.shape[2]
    groups_here = sequence.shape[1] // per_group
    first = lax.axis_index("sp") * groups_here
    pick = lambda table: lax.dynamic_slice_in_dim(table, first, groups_here, 0)
    factors = step_factors(
        pick(lam_real), pick(lam_imag), pick(log_step), pick(b_real), pick(b_imag)
    )
    direct = lax.dynamic_slice_in_dim(skip_weight, first * per_group, groups_here * per_group, 0)
    zeros = jnp.zeros((factors[0].size,), jnp.float32)
    return run_blocks(sequence, factors, pick(c_real), pick(c_imag), direct, (zeros, zeros))


def shards(
    hidden_in,
    in_weight,
    lam_real,
    lam_imag,
    log_step,
    b_real,
    b_imag,
    c_real,
    c_imag,
    skip_weight,
    lin_weight,
    gate_weight,
):
    tok_rows = hidden_in[0]
    inputs = jnp.dot(
        tok_rows,
        lax.all_gather(in_weight, ("sp", "dp"), axis=0, tiled=True),
        preferred_element_type=jnp.float32,
    ).astype(jnp.bfloat16)
    sequence = lax.all_to_all(inputs, "sp", split_axis=1, concat_axis=0, tiled=True)
    mixer_local = by_groups(
        sequence, lam_real, lam_imag, log_step, b_real, b_imag, c_real, c_imag, skip_weight
    )
    mixer_out = lax.all_to_all(mixer_local, "sp", split_axis=0, concat_axis=1, tiled=True)
    stacked = jnp.stack((lin_weight, gate_weight), 0)
    piece = lax.all_gather(stacked, ("sp", "dp"), axis=2, tiled=True)
    linear = jnp.dot(mixer_out, piece[0], preferred_element_type=jnp.float32)
    gate = jnp.dot(mixer_out, piece[1], preferred_element_type=jnp.float32)
    mixed = (linear * jax.nn.sigmoid(gate)).astype(jnp.bfloat16)
    return mixed[None]


def solution(mesh):
    placed = (
        P("dp", "sp", None),
        P(("sp", "dp"), None),
        P(),
        P(),
        P(),
        P(),
        P(),
        P(),
        P(),
        P(),
        P(None, ("sp", "dp")),
        P(None, ("sp", "dp")),
    )
    return jax.shard_map(
        shards, mesh=mesh, in_specs=placed, out_specs=P("dp", "sp", None), check_vma=False
    )
```

profile of v0, /device:TPU:0, one launch (start us, length us, event | category | flops | bytes accessed | tf_op | source)
XLA Modules:
  0.0 329.8 jit_solution(8766798775835108126)
XLA Ops:
  7.3 1.5 pad_maximum_fusion.32
  11.7 57.5 %all-gather.3.cloned.1.call-done = bf16[2048,512]{1,0:T(8,128)(2,1)} async-done(((bf16[64,512]{1,0:T(8,128)(2,1)}), bf16[2048,512]{1,0:T(8,128)(2,1)}) %all-gather.3.cloned.1.call-update) | async-done | bytes 2097168 | tf_op jit(solution)/shard_map/all_gather | solution.py:105
  69.2 2.0 convolution_convert_fusion
  72.0 4.3 %all-to-all-start = ((bf16[128,8,64]{0,2,1:T(8,128)(2,1)}), bf16[128,8,64]{0,2,1:T(8,128)(2,1)S(1)}, u32[]{:S(2)}, u32[]{:S(2)}) async-start(bf16[128,8,64]{0,2,1:T(8,128)(2,1)} %bitcast.30), calls=%async_computation | async-start | bytes 262144 | tf_op jit(solution)/shard_map/all_to_all | solution.py:108
  76.3 1.4 constant_dynamic-slice_fusion.1
  79.2 1.3 dynamic_slice.38
  80.5 1.4 multiply_add_fusion.9
  81.9 1.8 all-to-all-done
  85.7 220.2 %while.18 = (s32[]{:T(128)}, f32[256]{0:T(256)}, f32[256]{0:T(256)}, bf16[2,512,64]{1,2,0:T(8,128)(2,1)}, bf16[2,512,64]{1,2,0:T(8,128)(2,1)}, /*index=5*/f32[4,...) while((s32[]{:T(128)}, f32[256]{0:T(256)}, ...), condition=%wide.wide.region_1.2_spmd, body=%wide.wide.region_0.1_spmd.sunk | while | flops 107067392 | bytes 58788564 | solution.py:71
  86.7 1.2 fusion.68
  87.9 11.6 %slice.1808 = f32[255,256]{0,1:T(8,128)S(1)} slice(f32[512,256]{0,1:T(8,128)S(1)} %bitcast.175), slice={[2:512:2], [0:256:1]} | slice | bytes 522240 | tf_op jit(solution)/shard_map/while/body/eval_jaxpr/slice | solution.py:47
  99.7 11.7 %slice.1809 = f32[256,256]{0,1:T(8,128)S(1)} slice(f32[512,256]{0,1:T(8,128)S(1)} %bitcast.176), slice={[1:512:2], [0:256:1]} | slice | bytes 524288 | tf_op jit(solution)/shard_map/while/body/eval_jaxpr/slice | solution.py:47
  111.5 1.2 fusion.69
  112.7 11.7 %slice.1810 = f32[256,256]{0,1:T(8,128)S(1)} slice(f32[512,256]{0,1:T(8,128)S(1)} %bitcast.171), slice={[0:511:2], [0:256:1]} | slice | bytes 524288 | tf_op jit(solution)/shard_map/while/body/eval_jaxpr/slice | solution.py:47
  124.5 11.7 %slice.1811 = f32[256,256]{0,1:T(8,128)S(1)} slice(f32[512,256]{0,1:T(8,128)S(1)} %bitcast.177), slice={[0:511:2], [0:256:1]} | slice | bytes 524288 | tf_op jit(solution)/shard_map/while/body/eval_jaxpr/slice | solution.py:47
  136.3 11.7 %slice.1812 = f32[256,256]{0,1:T(8,128)S(1)} slice(f32[512,256]{0,1:T(8,128)S(1)} %bitcast.172), slice={[1:512:2], [0:256:1]} | slice | bytes 524288 | tf_op jit(solution)/shard_map/while/body/eval_jaxpr/slice | solution.py:47
  153.8 11.6 %slice.1866 = f32[255,256]{0,1:T(8,128)S(1)} slice(f32[512,256]{0,1:T(8,128)S(1)} %bitcast.173), slice={[2:512:2], [0:256:1]} | slice | bytes 522240 | tf_op jit(solution)/shard_map/while/body/eval_jaxpr/slice | solution.py:47
  167.8 1.7 pad.1009
  170.8 1.4 multiply_subtract_fusion.38
  172.3 1.4 pad_maximum_fusion.120
  173.7 2.6 pad.1038
  177.0 2.7 pad.1039
  180.7 1.7 pad.1040
  183.1 2.6 pad.1041
  185.9 1.8 pad.1042
  187.7 1.7 pad.1043
  189.5 2.0 multiply_add_fusion.34
  196.9 1.2 fusion.68
  198.0 11.6 %slice.1808 = f32[255,256]{0,1:T(8,128)S(1)} slice(f32[512,256]{0,1:T(8,128)S(1)} %bitcast.175), slice={[2:512:2], [0:256:1]} | slice | bytes 522240 | tf_op jit(solution)/shard_map/while/body/eval_jaxpr/slice | solution.py:47
  209.8 11.7 %slice.1809 = f32[256,256]{0,1:T(8,128)S(1)} slice(f32[512,256]{0,1:T(8,128)S(1)} %bitcast.176), slice={[1:512:2], [0:256:1]} | slice | bytes 524288 | tf_op jit(solution)/shard_map/while/body/eval_jaxpr/slice | solution.py:47
  221.6 1.2 fusion.69
  222.8 11.7 %slice.1810 = f32[256,256]{0,1:T(8,128)S(1)} slice(f32[512,256]{0,1:T(8,128)S(1)} %bitcast.171), slice={[0:511:2], [0:256:1]} | slice | bytes 524288 | tf_op jit(solution)/shard_map/while/body/eval_jaxpr/slice | solution.py:47
  234.6 11.7 %slice.1811 = f32[256,256]{0,1:T(8,128)S(1)} slice(f32[512,256]{0,1:T(8,128)S(1)} %bitcast.177), slice={[0:511:2], [0:256:1]} | slice | bytes 524288 | tf_op jit(solution)/shard_map/while/body/eval_jaxpr/slice | solution.py:47
  246.4 11.7 %slice.1812 = f32[256,256]{0,1:T(8,128)S(1)} slice(f32[512,256]{0,1:T(8,128)S(1)} %bitcast.172), slice={[1:512:2], [0:256:1]} | slice | bytes 524288 | tf_op jit(solution)/shard_map/while/body/eval_jaxpr/slice | solution.py:47
  263.9 11.6 %slice.1866 = f32[255,256]{0,1:T(8,128)S(1)} slice(f32[512,256]{0,1:T(8,128)S(1)} %bitcast.173), slice={[2:512:2], [0:256:1]} | slice | bytes 522240 | tf_op jit(solution)/shard_map/while/body/eval_jaxpr/slice | solution.py:47
  278.0 1.7 pad.1009
  281.0 1.4 multiply_subtract_fusion.38
  282.4 1.4 pad_maximum_fusion.120
  283.8 2.6 pad.1038
  287.2 2.7 pad.1039
  290.8 1.7 pad.1040
  293.2 2.6 pad.1041
  296.1 1.8 pad.1042
  297.9 1.7 pad.1043
  299.6 2.0 multiply_add_fusion.34
  307.2 11.3 %all_to_all.35 = bf16[8,128,64]{1,2,0:T(8,128)(2,1)S(1)} all-to-all(bf16[8,128,64]{1,2,0:T(8,128)(2,1)S(1)} %copy.53), channel_id=1, replica_groups=mesh['sp'=8,'dp'=4] {'sp'}, dimensions={0} | all-to-all | bytes 262144 | tf_op jit(solution)/shard_map/all_to_all | solution.py:112
  318.5 2.6 fusion.15
  321.3 1.6 fusion.17
  (698 shorter events, 41.8 us)
Async XLA Ops:
  6.5 62.7 %copy-start = (bf16[1,128,2048]{2,1,0:T(8,128)(2,1)S(1)}, bf16[1,128,2048]{2,1,0:T(8,128)(2,1)}, u32[]{:S(2)}) copy-start(bf16[1,128,2048]{2,1,0:T(8,128)(2,1)} %param.14) | copy-start | bytes 1572868
  6.5 62.7 %all-gather.3.cloned.1.call-start = ((), (), s32[]{:S(2)}) async-start(), calls=%async_computation.2 | async-start | bytes 2162688 | tf_op jit(solution)/shard_map/all_gather | solution.py:105
  7.3 311.2 %all-gather.5.cloned.1.call-start = ((), (), s32[]{:S(2)}) async-start(), calls=%async_computation.3 | async-start | bytes 4325376 | tf_op jit(solution)/shard_map/all_gather | solution.py:114
  10.4 68.0 %copy-start.59 = (f32[4,64]{1,0:T(4,128)}, f32[4,64]{1,0:T(4,128)S(1)}, u32[]{:S(2)}) copy-start(f32[4,64]{1,0:T(4,128)S(1)} %get-tuple-element.1164) | copy-start | bytes 3076
  10.5 74.1 %copy-start.62 = (f32[4,64]{1,0:T(4,128)}, f32[4,64]{1,0:T(4,128)S(1)}, u32[]{:S(2)}) copy-start(f32[4,64]{1,0:T(4,128)S(1)} %get-tuple-element.1163) | copy-start | bytes 3076
  72.0 11.7 %all-to-all-start = ((bf16[128,8,64]{0,2,1:T(8,128)(2,1)}), bf16[128,8,64]{0,2,1:T(8,128)(2,1)S(1)}, u32[]{:S(2)}, u32[]{:S(2)}) async-start(bf16[128,8,64]{0,2,1:T(8,128)(2,1)} %bitcast.30), calls=%async_computation | async-start | bytes 262144 | tf_op jit(solution)/shard_map/all_to_all | solution.py:108
  85.7 63.1 %copy-start.36 = (f32[256]{0:T(256)}, f32[256]{0:T(256)S(1)}, u32[]{:S(2)}) copy-start(f32[256]{0:T(256)S(1)} %get-tuple-element.1259) | copy-start | bytes 3076 | tf_op jit(solution)/shard_map/while
  85.7 63.1 %copy-start.39 = (f32[256]{0:T(256)}, f32[256]{0:T(256)S(1)}, u32[]{:S(2)}) copy-start(f32[256]{0:T(256)S(1)} %get-tuple-element.1260) | copy-start | bytes 3076 | tf_op jit(solution)/shard_map/while
  85.8 65.3 %copy-start.44 = (f32[256]{0:T(256)}, f32[256]{0:T(256)S(1)}, u32[]{:S(2)}) copy-start(f32[256]{0:T(256)S(1)} %get-tuple-element.1252) | copy-start | bytes 3076 | tf_op jit(solution)/shard_map/while
  85.8 65.3 %copy-start.47 = (f32[1,256]{1,0:T(1,128)}, f32[1,256]{1,0:T(1,128)S(1)}, u32[]{:S(2)}) copy-start(f32[1,256]{1,0:T(1,128)S(1)} %get-tuple-element.1255) | copy-start | bytes 3076 | tf_op jit(solution)/shard_map/while
  85.8 65.3 %copy-start.50 = (f32[1,256]{1,0:T(1,128)}, f32[1,256]{1,0:T(1,128)S(1)}, u32[]{:S(2)}) copy-start(f32[1,256]{1,0:T(1,128)S(1)} %get-tuple-element.1254) | copy-start | bytes 3076 | tf_op jit(solution)/shard_map/while
  85.8 65.3 %copy-start.53 = (f32[256]{0:T(256)}, f32[256]{0:T(256)S(1)}, u32[]{:S(2)}) copy-start(f32[256]{0:T(256)S(1)} %get-tuple-element.1253) | copy-start | bytes 3076 | tf_op jit(solution)/shard_map/while
  85.8 66.1 %copy-start.30 = (f32[256]{0:T(256)}, f32[256]{0:T(256)S(1)}, u32[]{:S(2)}) copy-start(f32[256]{0:T(256)S(1)} %get-tuple-element.1249) | copy-start | bytes 3076 | tf_op jit(solution)/shard_map/while
  85.8 66.1 %copy-start.33 = (f32[256]{0:T(256)}, f32[256]{0:T(256)S(1)}, u32[]{:S(2)}) copy-start(f32[256]{0:T(256)S(1)} %get-tuple-element.1248) | copy-start | bytes 3076 | tf_op jit(solution)/shard_map/while
  85.8 66.3 %copy-start.24 = (f32[256]{0:T(256)}, f32[256]{0:T(256)S(1)}, u32[]{:S(2)}) copy-start(f32[256]{0:T(256)S(1)} %get-tuple-element.1247) | copy-start | bytes 3076 | tf_op jit(solution)/shard_map/while
  85.8 66.3 %copy-start.27 = (f32[256]{0:T(256)}, f32[256]{0:T(256)S(1)}, u32[]{:S(2)}) copy-start(f32[256]{0:T(256)S(1)} %get-tuple-element.1246) | copy-start | bytes 3076 | tf_op jit(solution)/shard_map/while
  85.8 66.4 %copy-start.18 = (f32[256]{0:T(256)}, f32[256]{0:T(256)S(1)}, u32[]{:S(2)}) copy-start(f32[256]{0:T(256)S(1)} %get-tuple-element.1245) | copy-start | bytes 3076 | tf_op jit(solution)/shard_map/while
  85.8 66.4 %copy-start.21 = (f32[256]{0:T(256)}, f32[256]{0:T(256)S(1)}, u32[]{:S(2)}) copy-start(f32[256]{0:T(256)S(1)} %get-tuple-element.1244) | copy-start | bytes 3076 | tf_op jit(solution)/shard_map/while
  85.8 66.6 %copy-start.6 = (f32[256]{0:T(256)}, f32[256]{0:T(256)S(1)}, u32[]{:S(2)}) copy-start(f32[256]{0:T(256)S(1)} %get-tuple-element.1243) | copy-start | bytes 3076 | tf_op jit(solution)/shard_map/while
  85.8 66.6 %copy-start.9 = (f32[256]{0:T(256)}, f32[256]{0:T(256)S(1)}, u32[]{:S(2)}) copy-start(f32[256]{0:T(256)S(1)} %get-tuple-element.1242) | copy-start | bytes 3076 | tf_op jit(solution)/shard_map/while
  85.9 66.8 %copy-start.12 = (f32[256]{0:T(256)}, f32[256]{0:T(256)S(1)}, u32[]{:S(2)}) copy-start(f32[256]{0:T(256)S(1)} %get-tuple-element.1241) | copy-start | bytes 3076 | tf_op jit(solution)/shard_map/while
  85.9 66.8 %copy-start.15 = (f32[256]{0:T(256)}, f32[256]{0:T(256)S(1)}, u32[]{:S(2)}) copy-start(f32[256]{0:T(256)S(1)} %get-tuple-element.1240) | copy-start | bytes 3076 | tf_op jit(solution)/shard_map/while
  153.6 12.7 %copy-start.37 = (f32[256]{0:T(256)S(1)}, f32[256]{0:T(256)}, u32[]{:S(2)}) copy-start(f32[256]{0:T(256)} %copy-done.36) | copy-start | bytes 3076 | tf_op jit(solution)/shard_map/while
  153.6 12.7 %copy-start.40 = (f32[256]{0:T(256)S(1)}, f32[256]{0:T(256)}, u32[]{:S(2)}) copy-start(f32[256]{0:T(256)} %copy-done.39) | copy-start | bytes 3076 | tf_op jit(solution)/shard_map/while
  170.8 8.9 %copy-start.58 = (f32[1,256]{1,0:T(1,128)S(1)}, f32[1,256]{1,0:T(1,128)}, u32[]{:S(2)}) copy-start(f32[1,256]{1,0:T(1,128)} %get-tuple-element.1262) | copy-start | bytes 3076 | tf_op jit(solution)/shard_map/while
  183.1 6.4 %copy-start.60 = (f32[256]{0:T(256)S(1)}, f32[256]{0:T(256)}, u32[]{:S(2)}) copy-start(f32[256]{0:T(256)} %get-tuple-element.1194) | copy-start | bytes 3076 | tf_op jit(solution)/shard_map/while
  183.1 6.4 %copy-start.61 = (f32[256]{0:T(256)S(1)}, f32[256]{0:T(256)}, u32[]{:S(2)}) copy-start(f32[256]{0:T(256)} %get-tuple-element.1195) | copy-start | bytes 3076 | tf_op jit(solution)/shard_map/while
  195.9 63.1 %copy-start.36 = (f32[256]{0:T(256)}, f32[256]{0:T(256)S(1)}, u32[]{:S(2)}) copy-start(f32[256]{0:T(256)S(1)} %get-tuple-element.1259) | copy-start | bytes 3076 | tf_op jit(solution)/shard_map/while
  195.9 63.1 %copy-start.39 = (f32[256]{0:T(256)}, f32[256]{0:T(256)S(1)}, u32[]{:S(2)}) copy-start(f32[256]{0:T(256)S(1)} %get-tuple-element.1260) | copy-start | bytes 3076 | tf_op jit(solution)/shard_map/while
  195.9 65.3 %copy-start.44 = (f32[256]{0:T(256)}, f32[256]{0:T(256)S(1)}, u32[]{:S(2)}) copy-start(f32[256]{0:T(256)S(1)} %get-tuple-element.1252) | copy-start | bytes 3076 | tf_op jit(solution)/shard_map/while
  195.9 65.3 %copy-start.47 = (f32[1,256]{1,0:T(1,128)}, f32[1,256]{1,0:T(1,128)S(1)}, u32[]{:S(2)}) copy-start(f32[1,256]{1,0:T(1,128)S(1)} %get-tuple-element.1255) | copy-start | bytes 3076 | tf_op jit(solution)/shard_map/while
  195.9 65.3 %copy-start.50 = (f32[1,256]{1,0:T(1,128)}, f32[1,256]{1,0:T(1,128)S(1)}, u32[]{:S(2)}) copy-start(f32[1,256]{1,0:T(1,128)S(1)} %get-tuple-element.1254) | copy-start | bytes 3076 | tf_op jit(solution)/shard_map/while
  195.9 65.3 %copy-start.53 = (f32[256]{0:T(256)}, f32[256]{0:T(256)S(1)}, u32[]{:S(2)}) copy-start(f32[256]{0:T(256)S(1)} %get-tuple-element.1253) | copy-start | bytes 3076 | tf_op jit(solution)/shard_map/while
  195.9 66.1 %copy-start.30 = (f32[256]{0:T(256)}, f32[256]{0:T(256)S(1)}, u32[]{:S(2)}) copy-start(f32[256]{0:T(256)S(1)} %get-tuple-element.1249) | copy-start | bytes 3076 | tf_op jit(solution)/shard_map/while
  195.9 66.1 %copy-start.33 = (f32[256]{0:T(256)}, f32[256]{0:T(256)S(1)}, u32[]{:S(2)}) copy-start(f32[256]{0:T(256)S(1)} %get-tuple-element.1248) | copy-start | bytes 3076 | tf_op jit(solution)/shard_map/while
  195.9 66.3 %copy-start.24 = (f32[256]{0:T(256)}, f32[256]{0:T(256)S(1)}, u32[]{:S(2)}) copy-start(f32[256]{0:T(256)S(1)} %get-tuple-element.1247) | copy-start | bytes 3076 | tf_op jit(solution)/shard_map/while
  195.9 66.3 %copy-start.27 = (f32[256]{0:T(256)}, f32[256]{0:T(256)S(1)}, u32[]{:S(2)}) copy-start(f32[256]{0:T(256)S(1)} %get-tuple-element.1246) | copy-start | bytes 3076 | tf_op jit(solution)/shard_map/while
  196.0 66.4 %copy-start.18 = (f32[256]{0:T(256)}, f32[256]{0:T(256)S(1)}, u32[]{:S(2)}) copy-start(f32[256]{0:T(256)S(1)} %get-tuple-element.1245) | copy-start | bytes 3076 | tf_op jit(solution)/shard_map/while
  196.0 66.4 %copy-start.21 = (f32[256]{0:T(256)}, f32[256]{0:T(256)S(1)}, u32[]{:S(2)}) copy-start(f32[256]{0:T(256)S(1)} %get-tuple-element.1244) | copy-start | bytes 3076 | tf_op jit(solution)/shard_map/while
  196.0 66.6 %copy-start.6 = (f32[256]{0:T(256)}, f32[256]{0:T(256)S(1)}, u32[]{:S(2)}) copy-start(f32[256]{0:T(256)S(1)} %get-tuple-element.1243) | copy-start | bytes 3076 | tf_op jit(solution)/shard_map/while
  196.0 66.6 %copy-start.9 = (f32[256]{0:T(256)}, f32[256]{0:T(256)S(1)}, u32[]{:S(2)}) copy-start(f32[256]{0:T(256)S(1)} %get-tuple-element.1242) | copy-start | bytes 3076 | tf_op jit(solution)/shard_map/while
  196.0 66.8 %copy-start.12 = (f32[256]{0:T(256)}, f32[256]{0:T(256)S(1)}, u32[]{:S(2)}) copy-start(f32[256]{0:T(256)S(1)} %get-tuple-element.1241) | copy-start | bytes 3076 | tf_op jit(solution)/shard_map/while
  196.0 66.8 %copy-start.15 = (f32[256]{0:T(256)}, f32[256]{0:T(256)S(1)}, u32[]{:S(2)}) copy-start(f32[256]{0:T(256)S(1)} %get-tuple-element.1240) | copy-start | bytes 3076 | tf_op jit(solution)/shard_map/while
  263.7 12.7 %copy-start.37 = (f32[256]{0:T(256)S(1)}, f32[256]{0:T(256)}, u32[]{:S(2)}) copy-start(f32[256]{0:T(256)} %copy-done.36) | copy-start | bytes 3076 | tf_op jit(solution)/shard_map/while
  263.7 12.7 %copy-start.40 = (f32[256]{0:T(256)S(1)}, f32[256]{0:T(256)}, u32[]{:S(2)}) copy-start(f32[256]{0:T(256)} %copy-done.39) | copy-start | bytes 3076 | tf_op jit(solution)/shard_map/while
  280.9 8.9 %copy-start.58 = (f32[1,256]{1,0:T(1,128)S(1)}, f32[1,256]{1,0:T(1,128)}, u32[]{:S(2)}) copy-start(f32[1,256]{1,0:T(1,128)} %get-tuple-element.1262) | copy-start | bytes 3076 | tf_op jit(solution)/shard_map/while
  293.2 6.4 %copy-start.60 = (f32[256]{0:T(256)S(1)}, f32[256]{0:T(256)}, u32[]{:S(2)}) copy-start(f32[256]{0:T(256)} %get-tuple-element.1194) | copy-start | bytes 3076 | tf_op jit(solution)/shard_map/while
  293.2 6.4 %copy-start.61 = (f32[256]{0:T(256)S(1)}, f32[256]{0:T(256)}, u32[]{:S(2)}) copy-start(f32[256]{0:T(256)} %get-tuple-element.1195) | copy-start | bytes 3076 | tf_op jit(solution)/shard_map/while
  (79 other events, 278.2 us)
Sparse Core Ops, SparseCore 0:
  10.2 58.9 all-gather.2
  72.1 60.4 all-gather.4
where the time goes:
time: 331 us; the launch traced here: 330 us
  local copies, waits for them, and re-layouts  195 us (59%)
  waiting for transfers between devices  60.1 us (18%)
  other arithmetic  28.5 us (9%)
  between operations  13.5 us (4%)
  matrix products  12.5 us (4%)
  blocking collectives  11.3 us (3%)
  starting transfers between devices  4.36 us (1%)
  loops' own time  3.98 us (1%)
    slice x128, local copies, waits for them, and re-layouts, block_scan(): lax.associative_scan(combine, (are, aim, drive_re, drive_im), axis=0)  145 us
    all_gather x1, waiting for transfers between devices, shards(): lax.all_gather(in_weight, ('sp', 'dp'), axis=0, tiled=True)  57.5 us
    pad x128, local copies, waits for them, and re-layouts, block_scan(): lax.associative_scan(combine, (are, aim, drive_re, drive_im), axis=0)  31.2 us
    all_to_all x1, blocking collectives, shards(): lax.all_to_all(mixer_local, 'sp', split_axis=0, concat_axis=1, tiled=True)  11.3 us
  transfers between devices with their start and end apart: 3, of which 2 were waited for; matrix products, arithmetic and copies ran while one was open for 70% of the time, Pallas kernels for 0%

commit v1 on v0

v1 whole, which is shorter than its diff:
```python
import functools

import jax
import jax.numpy as jnp
from jax import lax
from jax.experimental import pallas as pl
from jax.experimental.pallas import tpu as pltpu
from jax.sharding import PartitionSpec as P

MESH = pl.DeviceIdType.MESH
LANES = 128
SUBLANES = 8
CORES = 2


def step_factors(lam_real, lam_imag, log_step):
    step = jnp.exp(log_step)[:, None]
    xpart = lam_real * step
    wpart = lam_imag * step
    decay_re = jnp.exp(xpart) * jnp.cos(wpart)
    decay_im = jnp.exp(xpart) * jnp.sin(wpart)
    numer_re = jnp.expm1(xpart) * jnp.cos(wpart) - 2.0 * jnp.sin(0.5 * wpart) ** 2
    magnitude = lam_real * lam_real + lam_imag * lam_imag
    ratio_re = (numer_re * lam_real + decay_im * lam_imag) / magnitude
    ratio_im = (decay_im * lam_real - numer_re * lam_imag) / magnitude
    return decay_re, decay_im, ratio_re, ratio_im


def cmul(a, b):
    return a[0] * b[0] - a[1] * b[1], a[0] * b[1] + a[1] * b[0]


def cpow(a, power):
    result = None
    while power:
        if power & 1:
            result = a if result is None else cmul(result, a)
        power >>= 1
        if power:
            a = cmul(a, a)
    return result


def split(value):
    high = value.astype(jnp.bfloat16)
    return high, (value - high.astype(jnp.float32)).astype(jnp.bfloat16)


def nn(a, b):
    return jnp.dot(a, b, preferred_element_type=jnp.float32)


def nt(a, b):
    return lax.dot_general(a, b, (((1,), (1,)), ((), ())), preferred_element_type=jnp.float32)


def kernel(
    sizes,
    x_ref,
    win_ref,
    wout_ref,
    factor_ref,
    bmat_ref,
    cmat_ref,
    skip_ref,
    out_ref,
    win,
    wout,
    blocks,
    drive,
    ends,
    edge,
    mine,
    others,
    inner,
    send_z,
    recv_z,
    send_a,
    recv_a,
    send_b,
    recv_b,
    send_c,
    recv_c,
    send_e,
    recv_e,
):
    sp, dp = sizes
    n = dp // CORES
    nz = sp // n
    sp_me, dp_me = lax.axis_index("sp"), lax.axis_index("dp")
    z, x = sp_me // n, sp_me % n
    y, core = dp_me // CORES, dp_me % CORES
    rows = win_ref.shape[0]
    cols = wout_ref.shape[1]
    tokens, width = x_ref.shape
    channels = win_ref.shape[1]
    heads, lanes = bmat_ref.shape[1:]
    steps = tokens // SUBLANES

    def place(dz, a, b):
        zz = (z + dz) % nz
        xx = (x + a * (1 - core) + b * core) % n
        yy = (y + b * (1 - core) + a * core) % n
        return zz * n + xx, yy * CORES + core

    def owner(dz, a, b, c):
        zz = (z + nz - dz) % nz
        xx = (x + n - (a * (1 - c) + b * c)) % n
        yy = (y + n - (b * (1 - c) + a * c)) % n
        return (zz * n + xx) * dp + yy * CORES + c

    partner = (sp_me, y * CORES + (1 - core))

    def slot(w, index):
        if w == 0:
            return win.at[pl.ds(pl.multiple_of(index * rows, rows), rows), :]
        return wout.at[:, pl.ds(pl.multiple_of(index * cols, cols), cols), :]

    def copy(w, dz, a, b, c, target, sems, where, own=False):
        index = owner(dz, a, b, c)
        there = slot(w, index)
        source = (win_ref, wout_ref)[w] if own else there
        spot = (w,) + where
        return pltpu.make_async_remote_copy(
            src_ref=source,
            dst_ref=there,
            send_sem=sems[0].at[spot],
            recv_sem=sems[1].at[spot],
            device_id=target,
            device_id_type=MESH,
        )

    zs, as_, bs, cs = (send_z, recv_z), (send_a, recv_a), (send_b, recv_b), (send_c, recv_c)

    def copy_z(w, dz):
        return copy(w, 0, 0, 0, core, place(dz, 0, 0), zs, (dz - 1,), own=True)

    def copy_a(w, a, dz):
        return copy(w, dz, 0, 0, core, place(0, a, 0), as_, (a - 1, dz), own=dz == 0)

    def copy_b(w, b, a, dz):
        return copy(w, dz, a, 0, core, place(0, 0, b), bs, (b - 1, a, dz), own=dz == 0 and a == 0)

    def copy_c(w, b, a, dz):
        return copy(w, dz, a, b, core, partner, cs, (b, a, dz), own=dz == 0 and a == 0 and b == 0)

    def arrive_z(w, dz):
        copy(w, dz, 0, 0, core, partner, zs, (dz - 1,)).wait_recv()

    def arrive_a(w, a, dz):
        copy(w, dz, a, 0, core, partner, as_, (a - 1, dz)).wait_recv()

    def arrive_b(w, b, a, dz):
        copy(w, dz, a, b, core, partner, bs, (b - 1, a, dz)).wait_recv()

    def arrive_c(w, b, a, dz):
        copy(w, dz, a, b, 1 - core, partner, cs, (b, a, dz)).wait_recv()

    def pass_b(w, a, dz):
        for b in range(1, n):
            copy_b(w, b, a, dz).start()
        copy_c(w, 0, a, dz).start()

    def pass_a(w, dz):
        for a in range(1, n):
            copy_a(w, a, dz).start()
        pass_b(w, 0, dz)

    def phase_own(w):
        for dz in range(1, nz):
            copy_z(w, dz).start()
        pass_a(w, 0)

    def phase_z(w):
        for dz in range(1, nz):
            arrive_z(w, dz)
            pass_a(w, dz)

    def phase_a(w):
        for a in range(1, n):
            for dz in range(nz):
                arrive_a(w, a, dz)
                pass_b(w, a, dz)

    def phase_b(w):
        for b in range(1, n):
            for a in range(n):
                for dz in range(nz):
                    arrive_b(w, b, a, dz)
                    copy_c(w, b, a, dz).start()

    def phase_c(w):
        for b in range(n):
            for a in range(n):
                for dz in range(nz):
                    arrive_c(w, b, a, dz)

    def close(w):
        for dz in range(1, nz):
            copy_z(w, dz).wait_send()
        for dz in range(nz):
            for a in range(n):
                if a > 0:
                    copy_a(w, a, dz).wait_send()
                for b in range(n):
                    if b > 0:
                        copy_b(w, b, a, dz).wait_send()
                    copy_c(w, b, a, dz).wait_send()

    barrier = pltpu.get_barrier_semaphore()
    greeted = [((sp_me + j) % sp, dp_me) for j in range(1, sp)]
    greeted += [(sp_me, (y + j) % n * CORES + core) for j in range(1, n)]
    greeted += [partner]
    for device in greeted:
        pl.semaphore_signal(barrier, inc=1, device_id=device, device_id_type=MESH)
    pl.semaphore_wait(barrier, len(greeted))

    phase_own(0)
    phase_own(1)
    home = sp_me * dp + dp_me
    win[pl.ds(pl.multiple_of(home * rows, rows), rows), :] = win_ref[...]
    wout[:, pl.ds(pl.multiple_of(home * cols, cols), cols), :] = wout_ref[...]
    phase_z(0)

    share = LANES // heads
    count = channels // LANES
    wide = lanes // count
    deep = wide // share

    def block(ref, part, i, base):
        piece = ref[part, :, i * wide : (i + 1) * wide]
        lane = lax.broadcasted_iota(jnp.int32, piece.shape, 1)
        stacked = [
            jnp.where((lane >= g * deep) & (lane < (g + 1) * deep), piece, 0.0)
            for g in range(share)
        ]
        high, low = split(jnp.concatenate(stacked, axis=0))
        blocks[base + 2 * part, i] = high
        blocks[base + 2 * part + 1, i] = low

    for i in range(count):
        for part in range(2):
            block(bmat_ref, part, i, 0)
    phase_a(0)
    for i in range(count):
        for part in range(2):
            block(cmat_ref, part, i, 4)
    phase_b(0)
    phase_z(1)
    phase_c(0)

    high_k = width // 4
    total = nn(x_ref[:, :high_k], win[:high_k, :])
    for i in range(1, 4):
        span = slice(i * high_k, (i + 1) * high_k)
        total += nn(x_ref[:, span], win[span, :])
    inputs = total.astype(jnp.bfloat16)

    r = lax.broadcasted_iota(jnp.int32, (tokens, tokens), 0)
    c = lax.broadcasted_iota(jnp.int32, (tokens, tokens), 1)
    order = lambda v: (v & (SUBLANES - 1)) * steps + lax.shift_right_logical(v, 3)
    mix = jnp.where(c == order(r), 1.0, 0.0).astype(jnp.bfloat16)
    back = jnp.where(r == order(c), 1.0, 0.0).astype(jnp.bfloat16)
    source = nn(mix, inputs)
    spread = source.astype(jnp.bfloat16)

    decay = (factor_ref[0:1, :], factor_ref[1:2, :])
    for i in range(count):
        span = slice(i * wide, (i + 1) * wide)
        piece = spread[:, i * LANES : (i + 1) * LANES]
        for part in range(2):
            drive[part, :, span] = nn(piece, blocks[2 * part, i]) + nn(piece, blocks[2 * part + 1, i])
        shape = (SUBLANES, wide)
        mul = (jnp.broadcast_to(decay[0][:, span], shape), jnp.broadcast_to(decay[1][:, span], shape))
        state = (drive[0, :SUBLANES, span], drive[1, :SUBLANES, span])
        for k in range(1, steps):
            at = slice(k * SUBLANES, (k + 1) * SUBLANES)
            moved = cmul(mul, state)
            state = (moved[0] + drive[0, at, span], moved[1] + drive[1, at, span])
        ends[0, :, span] = state[0]
        ends[1, :, span] = state[1]

    jump = cpow(decay, steps)
    carry = (ends[0, 0:1, :], ends[1, 0:1, :])
    for s in range(1, SUBLANES):
        moved = cmul(jump, carry)
        carry = (moved[0] + ends[0, s : s + 1, :], moved[1] + ends[1, s : s + 1, :])
    mine[0:1, :] = carry[0]
    mine[1:2, :] = carry[1]

    def exchange(j):
        return pltpu.make_async_remote_copy(
            src_ref=mine,
            dst_ref=others.at[j - 1],
            send_sem=send_e.at[j - 1],
            recv_sem=recv_e.at[j - 1],
            device_id=((sp_me + j) % sp, dp_me),
            device_id_type=MESH,
        )

    for j in range(1, sp):
        exchange(j).start()
    phase_a(1)
    phase_b(1)
    far = cpow(decay, tokens)
    carry = (jnp.zeros_like(decay[0]), jnp.zeros_like(decay[0]))
    for j in range(1, sp):
        exchange(j).wait_recv()
    for j in range(sp - 1, 0, -1):
        moved = cmul(far, carry)
        before = sp_me >= j
        carry = (
            jnp.where(before, moved[0] + others[j - 1, 0:1, :], 0.0),
            jnp.where(before, moved[1] + others[j - 1, 1:2, :], 0.0),
        )
    edge[0, 0:1, :] = carry[0]
    edge[1, 0:1, :] = carry[1]
    for s in range(1, SUBLANES):
        moved = cmul(jump, carry)
        carry = (moved[0] + ends[0, s - 1 : s, :], moved[1] + ends[1, s - 1 : s, :])
        edge[0, s : s + 1, :] = carry[0]
        edge[1, s : s + 1, :] = carry[1]

    for i in range(count):
        span = slice(i * wide, (i + 1) * wide)
        shape = (SUBLANES, wide)
        mul = (jnp.broadcast_to(decay[0][:, span], shape), jnp.broadcast_to(decay[1][:, span], shape))
        state = (edge[0, :, span], edge[1, :, span])
        for k in range(steps):
            at = slice(k * SUBLANES, (k + 1) * SUBLANES)
            moved = cmul(mul, state)
            state = (moved[0] + drive[0, at, span], moved[1] + drive[1, at, span])
            drive[0, at, span] = state[0]
            drive[1, at, span] = state[1]
        summed = []
        for part in range(2):
            high, low = split(drive[part, :, span])
            c_high, c_low = blocks[4 + 2 * part, i], blocks[5 + 2 * part, i]
            summed.append(nt(high, c_high) + (nt(low, c_high) + nt(high, c_low)))
        here = slice(i * LANES, (i + 1) * LANES)
        result = jax.nn.gelu(summed[0] - summed[1] + skip_ref[:, here] * source[:, here])
        inner[:, here] = result.astype(jnp.bfloat16)

    mixer_out = nn(back, inner[...]).astype(jnp.bfloat16)
    phase_c(1)
    tile = 2 * LANES
    for i in range(width // tile):
        span = slice(i * tile, (i + 1) * tile)
        linear = nt(mixer_out, wout[0, span, :])
        gate = nt(mixer_out, wout[1, span, :])
        out_ref[:, span] = (linear * jax.nn.sigmoid(gate)).astype(jnp.bfloat16)

    for j in range(1, sp):
        exchange(j).wait_send()
    close(0)
    close(1)


def shards(
    sizes,
    hidden_in,
    in_weight,
    lam_real,
    lam_imag,
    log_step,
    b_real,
    b_imag,
    c_real,
    c_imag,
    skip_weight,
    lin_weight,
    gate_weight,
):
    sp, dp = sizes
    n = dp // CORES
    nz = sp // n
    tokens, width = hidden_in.shape[1:]
    rows, channels = in_weight.shape
    groups, states, heads = b_real.shape
    lanes = groups * states
    decay_re, decay_im, ratio_re, ratio_im = step_factors(lam_real, lam_imag, log_step)
    factor = jnp.stack((decay_re.reshape(lanes), decay_im.reshape(lanes)), 0)
    bbar_re = ratio_re[..., None] * b_real - ratio_im[..., None] * b_imag
    bbar_im = ratio_re[..., None] * b_imag + ratio_im[..., None] * b_real
    bmat = jnp.stack((bbar_re, bbar_im), 0).transpose(0, 3, 1, 2).reshape(2, heads, lanes)
    cmat = jnp.stack((c_real, c_imag), 0).transpose(0, 2, 1, 3).reshape(2, heads, lanes)
    pieces = jnp.stack((lin_weight.T, gate_weight.T), 0)
    count = channels // LANES
    bf16, f32 = jnp.bfloat16, jnp.float32
    pair = lambda *shape: [pltpu.SemaphoreType.DMA(shape)] * 2
    mixed = pl.pallas_call(
        functools.partial(kernel, sizes),
        out_shape=jax.ShapeDtypeStruct((tokens, width), bf16),
        in_specs=[pl.BlockSpec(memory_space=pltpu.VMEM)] * 7,
        out_specs=pl.BlockSpec(memory_space=pltpu.VMEM),
        scratch_shapes=[
            pltpu.VMEM((rows * sp * dp, channels), bf16),
            pltpu.VMEM((2, width, channels), bf16),
            pltpu.VMEM((8, count, LANES, lanes // count), bf16),
            pltpu.VMEM((2, tokens, lanes), f32),
            pltpu.VMEM((2, SUBLANES, lanes), f32),
            pltpu.VMEM((2, SUBLANES, lanes), f32),
            pltpu.VMEM((2, lanes), f32),
            pltpu.VMEM((sp - 1, 2, lanes), f32),
            pltpu.VMEM((tokens, channels), bf16),
            *pair(2, nz - 1),
            *pair(2, n - 1, nz),
            *pair(2, n - 1, n, nz),
            *pair(2, n, n, nz),
            *pair(sp - 1),
        ],
        compiler_params=pltpu.CompilerParams(
            collective_id=0, has_side_effects=True, vmem_limit_bytes=60 * 1024 * 1024
        ),
    )(hidden_in[0], in_weight, pieces, factor, bmat, cmat, skip_weight[None])
    return mixed[None]


def solution(mesh):
    sizes = (mesh.shape["sp"], mesh.shape["dp"])
    placed = (
        P("dp", "sp", None),
        P(("sp", "dp"), None),
        P(),
        P(),
        P(),
        P(),
        P(),
        P(),
        P(),
        P(),
        P(None, ("sp", "dp")),
        P(None, ("sp", "dp")),
    )
    return jax.shard_map(
        functools.partial(shards, sizes),
        mesh=mesh,
        in_specs=placed,
        out_specs=P("dp", "sp", None),
        check_vma=False,
    )
```

time: 331 us -> 54.4 us (0.16)
  local copies, waits for them, and re-layouts: 195 us -> 4.81 us
  waiting for transfers between devices: 60.1 us -> 0 us
  Pallas kernels: 0 us -> 45.7 us
  other arithmetic: 28.5 us -> 3.41 us
  between operations: 13.5 us -> 0.08 us
  matrix products: 12.5 us -> 0 us
  blocking collectives: 11.3 us -> 0 us
  starting transfers between devices: 4.36 us -> 0 us
  loops' own time: 3.98 us -> 0 us
    slice x132 -> x0, local copies, waits for them, and re-layouts: 148 us -> none  [the longest x128 145 us: block_scan(): lax.associative_scan(combine, (are, aim, drive_re, drive_im), axis=0)]
    all_gather x2 -> x0, waiting for transfers between devices: 57.5 us -> none  [the longest x1 57.5 us: shards(): lax.all_gather(in_weight, ('sp', 'dp'), axis=0, tiled=True)]
    pallas_call x0 -> x1, Pallas kernels: none -> 45.7 us  [shards(): pl.pallas_call(functools.partial(kernel, sizes), out_shape=jax.ShapeDtype...]
    pad x128 -> x0, local copies, waits for them, and re-layouts: 31.2 us -> none  [block_scan(): lax.associative_scan(combine, (are, aim, drive_re, drive_im), axis=0)]
    add x111 -> x0, other arithmetic: 15.1 us -> none  [the longest x32 4.72 us: combine(): rre * lbim + rim * lbre + rbim]
    dot_general x11 -> x0, matrix products: 12.5 us -> none  [the longest x1 2.61 us: shards(): gate = jnp.dot(mixer_out, piece[1], preferred_element_type=jnp.float32)]
    all_to_all x1 -> x0, blocking collectives: 11.3 us -> none  [shards(): lax.all_to_all(mixer_local, 'sp', split_axis=0, concat_axis=1, tiled=True)]
    while x254 -> x0, local copies, waits for them, and re-layouts: 7.9 us -> none
  transfers between devices with their start and end apart: 3 -> 0, of which waited for: 2 -> 0; matrix products, arithmetic and copies ran while one was open for 70% -> 0% of each run, Pallas kernels for 0% -> 0%
where the time goes in v1:
time: 54.4 us; the launch traced here: 54 us
  Pallas kernels  45.7 us (84%)
  local copies, waits for them, and re-layouts  4.81 us (9%)
  other arithmetic  3.41 us (6%)
    pallas_call x1, Pallas kernels, shards(): pl.pallas_call(functools.partial(kernel, sizes), out_shape=jax.ShapeDtype...  45.7 us
    unnamed x9, local copies, waits for them, and re-layouts  1.91 us
    another operation x1, other arithmetic, shards(): jnp.stack((bbar_re, bbar_im), 0).transpose(0, 3, 1, 2)  1.1 us

profile of v1, /device:TPU:0, one launch (start us, length us, event | category | flops | bytes accessed | tf_op | source)
XLA Modules:
  0.0 54.0 jit_solution(15092969129588206885)
XLA Ops:
  0.0 0.7 %exp.7 = f32[32]{0:T(128)S(1)} exponential(f32[32]{0:T(128)} %param.16) | non-fusion elementwise | bytes 256 | tf_op jit(solution)/shard_map/exp | solution.py:17
  0.7 0.9 %fusion = (f32[32,64]{1,0:T(8,128)S(1)}, f32[32,64]{1,0:T(8,128)S(1)}, f32[32,64]{1,0:T(8,128)S(1)}, f32[32,64]{1,0:T(8,128)S(1)}) fusion(f32[32,64]{1,0:T(8,128)} %param.15, f32[32,64]{1,0:T(8,128)} %param.14, f32[32]{0:T(128)S(1)} %exp.7), kind=kLoop, calls=%fused_computation.8 | loop fusion | flops 40960 | bytes 49280 | tf_op jit(solution)/shard_map/div | solution.py:24
  1.6 1.1 %subtract_bitcast_fusion = (f32[1,32,64,16]{2,3,1,0:T(8,128)S(1)}, f32[1,32,64,16]{2,3,1,0:T(8,128)S(1)}) fusion(f32[32,64,16]{1,2,0:T(8,128)} %param.18, f32[32,64,16]{1,2,0:T(8,128)} %param.17, f32[32,64]{1,0:T(8,128)S(1)} %get-tuple-element.10, f32[32,64]{1,0:T(8,128)S(1)} %get-tuple-element.7), kind=kLoop, calls=%fused_computation.3 | loop fusion | flops 196608 | bytes 540672 | tf_op jit(solution)/shard_map/stack | solution.py:385
  2.8 0.2 copy.13
  2.9 0.0 copy-start
  2.9 0.0 copy-start.1
  3.0 0.9 %reshape.9.bmat_ref = f32[2,16,2048]{2,1,0:T(8,128)} reshape(f32[2,16,32,64]{3,2,1,0:T(8,128)S(1)} %copy.13) | data formatting | bytes 524288 | tf_op jit(solution)/shard_map/reshape | solution.py:385
  3.8 0.1 stack_reshape.6
  3.9 0.1 stack_reshape.7
  4.0 0.6 %pad_maximum_fusion.1.factor_ref = f32[2,2048]{1,0:T(2,128)} fusion(f32[1,2048]{1,0:T(1,128)S(1)} %stack_reshape.7, f32[1,2048]{1,0:T(1,128)S(1)} %stack_reshape.6), kind=kLoop, calls=%fused_computation.5 | loop fusion | flops 4096 | bytes 32768 | tf_op jit(solution)/shard_map/stack | solution.py:382
  4.6 0.0 copy-done
  4.6 0.0 copy-done.1
  4.7 0.2 copy.14
  4.8 0.0 copy-start.2
  4.8 0.0 copy-start.3
  4.9 0.9 %reshape.10.cmat_ref = f32[2,16,2048]{2,1,0:T(8,128)} reshape(f32[2,16,32,64]{3,2,1,0:T(8,128)S(1)} %copy.14) | data formatting | bytes 524288 | tf_op jit(solution)/shard_map/reshape | solution.py:386
  5.7 0.0 copy-done.2
  5.7 0.0 copy-done.3
  5.7 0.7 %pad_maximum_fusion.wout_ref = bf16[2,64,512]{2,1,0:T(8,128)(2,1)} fusion(bf16[1,64,512]{2,1,0:T(8,128)(2,1)S(1)} %bitcast.27, bf16[1,64,512]{2,1,0:T(8,128)(2,1)S(1)} %bitcast.28), kind=kLoop, calls=%fused_computation.4 | loop fusion | flops 65536 | bytes 262144 | tf_op jit(solution)/shard_map/stack | solution.py:387
  6.4 45.7 %shard_map.118 = bf16[128,2048]{1,0:T(8,128)(2,1)} custom-call(bf16[128,2048]{1,0:T(8,128)(2,1)} %bitcast.24, bf16[64,512]{1,0:T(8,128)(2,1)} %win_ref.1, bf16[2,64,512]{2,1,0:T(8,128)(2,1)} %pad_maximum_fusion.wout_ref, f32[2,2048]{1,0:T(2,128)} %pad_maximum_fusion.1.factor_ref, f32[2,16,2048]{2,1,0:T(8,128)} %reshape.9.bmat_ref, ...), custom_call_target="tpu_custom_call" | custom-call | tf_op jit(solution)/shard_map/pallas_call | solution.py:391
  52.1 1.9 %copy.16 = bf16[1,128,2048]{2,1,0:T(8,128)(2,1)} copy(bf16[1,128,2048]{2,1,0:T(8,128)(2,1)} %bitcast.23) | data formatting | bytes 1048576
  (2 shorter events, 0.1 us)
Async XLA Ops:
  2.9 1.7 %copy-start = (f32[32,16,64]{2,1,0:T(8,128)S(1)}, f32[32,16,64]{2,1,0:T(8,128)}, u32[]{:S(2)}) copy-start(f32[32,16,64]{2,1,0:T(8,128)} %param.20) | copy-start | bytes 393220
  2.9 1.7 %copy-start.1 = (f32[32,16,64]{2,1,0:T(8,128)S(1)}, f32[32,16,64]{2,1,0:T(8,128)}, u32[]{:S(2)}) copy-start(f32[32,16,64]{2,1,0:T(8,128)} %param.19) | copy-start | bytes 393220
  4.8 0.9 %copy-start.2 = (bf16[512,64]{0,1:T(8,128)(2,1)S(1)}, bf16[512,64]{0,1:T(8,128)(2,1)}, u32[]{:S(2)}) copy-start(bf16[512,64]{0,1:T(8,128)(2,1)} %param.23) | copy-start | bytes 196612
  4.8 0.9 %copy-start.3 = (bf16[512,64]{0,1:T(8,128)(2,1)S(1)}, bf16[512,64]{0,1:T(8,128)(2,1)}, u32[]{:S(2)}) copy-start(bf16[512,64]{0,1:T(8,128)(2,1)} %param.22) | copy-start | bytes 196612

commit v2 on v1

--- a/solution.py
+++ b/solution.py
@@ -13,13 +13,19 @@
 CORES = 2
 
 
-def step_factors(lam_real, lam_imag, log_step):
-    step = jnp.exp(log_step)[:, None]
+def expm1(value):
+    series = jnp.ones_like(value)
+    for k in range(11, 1, -1):
+        series = 1.0 + series * value * (1.0 / k)
+    return jnp.where(jnp.abs(value) < 0.5, value * series, jnp.exp(value) - 1.0)
+
+
+def step_factors(lam_real, lam_imag, step):
     xpart = lam_real * step
     wpart = lam_imag * step
     decay_re = jnp.exp(xpart) * jnp.cos(wpart)
     decay_im = jnp.exp(xpart) * jnp.sin(wpart)
-    numer_re = jnp.expm1(xpart) * jnp.cos(wpart) - 2.0 * jnp.sin(0.5 * wpart) ** 2
+    numer_re = expm1(xpart) * jnp.cos(wpart) - 2.0 * jnp.sin(0.5 * wpart) ** 2
     magnitude = lam_real * lam_real + lam_imag * lam_imag
     ratio_re = (numer_re * lam_real + decay_im * lam_imag) / magnitude
     ratio_im = (decay_im * lam_real - numer_re * lam_imag) / magnitude
@@ -59,14 +65,20 @@
     x_ref,
     win_ref,
     wout_ref,
-    factor_ref,
-    bmat_ref,
-    cmat_ref,
+    lam_re_ref,
+    lam_im_ref,
+    log_step_ref,
+    b_re_ref,
+    b_im_ref,
+    c_re_ref,
+    c_im_ref,
     skip_ref,
     out_ref,
     win,
     wout,
-    blocks,
+    tables,
+    factor,
+    compact,
     drive,
     ends,
     edge,
@@ -94,17 +106,29 @@
     cols = wout_ref.shape[1]
     tokens, width = x_ref.shape
     channels = win_ref.shape[1]
-    heads, lanes = bmat_ref.shape[1:]
+    groups, heads, states = c_re_ref.shape
+    lanes = groups * states
     steps = tokens // SUBLANES
 
+    def across(dz, sign):
+        if nz & (nz - 1):
+            return (z + nz + sign * dz) % nz
+        total = 0
+        bit = 1
+        while bit < nz:
+            held = z // bit % 2
+            total = total + bit * (1 - held if dz & bit else held)
+            bit *= 2
+        return total
+
     def place(dz, a, b):
-        zz = (z + dz) % nz
+        zz = across(dz, 1)
         xx = (x + a * (1 - core) + b * core) % n
         yy = (y + b * (1 - core) + a * core) % n
         return zz * n + xx, yy * CORES + core
 
     def owner(dz, a, b, c):
-        zz = (z + nz - dz) % nz
+        zz = across(dz, -1)
         xx = (x + n - (a * (1 - c) + b * c)) % n
         yy = (y + n - (b * (1 - c) + a * c)) % n
         return (zz * n + xx) * dp + yy * CORES + c
@@ -171,23 +195,34 @@
             copy_z(w, dz).start()
         pass_a(w, 0)
 
-    def phase_z(w):
-        for dz in range(1, nz):
-            arrive_z(w, dz)
-            pass_a(w, dz)
-
-    def phase_a(w):
-        for a in range(1, n):
-            for dz in range(nz):
-                arrive_a(w, a, dz)
-                pass_b(w, a, dz)
-
-    def phase_b(w):
-        for b in range(1, n):
-            for a in range(n):
-                for dz in range(nz):
-                    arrive_b(w, b, a, dz)
-                    copy_c(w, b, a, dz).start()
+    def step_z(w, dz):
+        arrive_z(w, dz)
+        pass_a(w, dz)
+
+    def step_a(w, a, dz):
+        arrive_a(w, a, dz)
+        pass_b(w, a, dz)
+
+    def step_b(w, b, a, dz):
+        arrive_b(w, b, a, dz)
+        copy_c(w, b, a, dz).start()
+
+    def line_up(w):
+        line = []
+        for t in range(nz + 2):
+            if 1 <= t < nz:
+                line.append((step_z, (w, t)))
+            if 0 <= t - 1 < nz:
+                line += [(step_a, (w, a, t - 1)) for a in range(1, n)]
+                line += [(step_b, (w, b, 0, t - 1)) for b in range(1, n)]
+            if 0 <= t - 2 < nz:
+                line += [(step_b, (w, b, a, t - 2)) for b in range(1, n) for a in range(1, n)]
+        return line
+
+    def take(line, most=1):
+        for _ in range(min(most, len(line))):
+            step, args = line.pop(0)
+            step(*args)
 
     def phase_c(w):
         for b in range(n):
@@ -220,33 +255,36 @@
     home = sp_me * dp + dp_me
     win[pl.ds(pl.multiple_of(home * rows, rows), rows), :] = win_ref[...]
     wout[:, pl.ds(pl.multiple_of(home * cols, cols), cols), :] = wout_ref[...]
-    phase_z(0)
+    first, second = line_up(0), line_up(1)
+    take(first, 2)
 
     share = LANES // heads
     count = channels // LANES
     wide = lanes // count
-    deep = wide // share
-
-    def block(ref, part, i, base):
-        piece = ref[part, :, i * wide : (i + 1) * wide]
-        lane = lax.broadcasted_iota(jnp.int32, piece.shape, 1)
-        stacked = [
-            jnp.where((lane >= g * deep) & (lane < (g + 1) * deep), piece, 0.0)
-            for g in range(share)
-        ]
-        high, low = split(jnp.concatenate(stacked, axis=0))
-        blocks[base + 2 * part, i] = high
-        blocks[base + 2 * part + 1, i] = low
-
+
+    step = jnp.exp(log_step_ref[...])
+    lam_re, lam_im = lam_re_ref[...], lam_im_ref[...]
+    decay_re, decay_im, ratio_re, ratio_im = step_factors(lam_re, lam_im, step)
+    for row, table in enumerate((decay_re, decay_im, ratio_re, ratio_im)):
+        for g in range(groups):
+            factor[row : row + 1, g * states : (g + 1) * states] = table[g : g + 1, :]
+    take(first, 2)
+    for part, ref in enumerate((b_re_ref, b_im_ref, c_re_ref, c_im_ref)):
+        for g in range(groups):
+            compact[part, :, g * states : (g + 1) * states] = ref[g]
+    take(first, 2)
+    lane = lax.broadcasted_iota(jnp.int32, (heads, wide), 1)
     for i in range(count):
-        for part in range(2):
-            block(bmat_ref, part, i, 0)
-    phase_a(0)
-    for i in range(count):
-        for part in range(2):
-            block(cmat_ref, part, i, 4)
-    phase_b(0)
-    phase_z(1)
+        for part in range(4):
+            for level, value in enumerate(split(compact[part, :, i * wide : (i + 1) * wide])):
+                for g in range(share):
+                    inside = (lane >= g * states) & (lane < (g + 1) * states)
+                    kept = jnp.where(inside, value, jnp.zeros_like(value))
+                    tables[2 * part + level, i, g * heads : (g + 1) * heads, :] = kept
+            if part % 2:
+                take(first, 1)
+    take(first, len(first))
+    take(second, 2)
     phase_c(0)
 
     high_k = width // 4
@@ -254,6 +292,7 @@
     for i in range(1, 4):
         span = slice(i * high_k, (i + 1) * high_k)
         total += nn(x_ref[:, span], win[span, :])
+        take(second, 1)
     inputs = total.astype(jnp.bfloat16)
 
     r = lax.broadcasted_iota(jnp.int32, (tokens, tokens), 0)
@@ -264,12 +303,15 @@
     source = nn(mix, inputs)
     spread = source.astype(jnp.bfloat16)
 
-    decay = (factor_ref[0:1, :], factor_ref[1:2, :])
+    decay = (factor[0:1, :], factor[1:2, :])
+    ratio = (factor[2:3, :], factor[3:4, :])
     for i in range(count):
         span = slice(i * wide, (i + 1) * wide)
         piece = spread[:, i * LANES : (i + 1) * LANES]
-        for part in range(2):
-            drive[part, :, span] = nn(piece, blocks[2 * part, i]) + nn(piece, blocks[2 * part + 1, i])
+        fed = tuple(nn(piece, tables[2 * part, i]) + nn(piece, tables[2 * part + 1, i]) for part in range(2))
+        fed = cmul((ratio[0][:, span], ratio[1][:, span]), fed)
+        drive[0, :, span] = fed[0]
+        drive[1, :, span] = fed[1]
         shape = (SUBLANES, wide)
         mul = (jnp.broadcast_to(decay[0][:, span], shape), jnp.broadcast_to(decay[1][:, span], shape))
         state = (drive[0, :SUBLANES, span], drive[1, :SUBLANES, span])
@@ -279,6 +321,7 @@
             state = (moved[0] + drive[0, at, span], moved[1] + drive[1, at, span])
         ends[0, :, span] = state[0]
         ends[1, :, span] = state[1]
+        take(second, 1)
 
     jump = cpow(decay, steps)
     carry = (ends[0, 0:1, :], ends[1, 0:1, :])
@@ -300,8 +343,7 @@
 
     for j in range(1, sp):
         exchange(j).start()
-    phase_a(1)
-    phase_b(1)
+    take(second, 2)
     far = cpow(decay, tokens)
     carry = (jnp.zeros_like(decay[0]), jnp.zeros_like(decay[0]))
     for j in range(1, sp):
@@ -335,13 +377,15 @@
         summed = []
         for part in range(2):
             high, low = split(drive[part, :, span])
-            c_high, c_low = blocks[4 + 2 * part, i], blocks[5 + 2 * part, i]
+            c_high, c_low = tables[4 + 2 * part, i], tables[5 + 2 * part, i]
             summed.append(nt(high, c_high) + (nt(low, c_high) + nt(high, c_low)))
         here = slice(i * LANES, (i + 1) * LANES)
         result = jax.nn.gelu(summed[0] - summed[1] + skip_ref[:, here] * source[:, here])
         inner[:, here] = result.astype(jnp.bfloat16)
+        take(second, 1)
 
     mixer_out = nn(back, inner[...]).astype(jnp.bfloat16)
+    take(second, len(second))
     phase_c(1)
     tile = 2 * LANES
     for i in range(width // tile):
@@ -378,12 +422,6 @@
     rows, channels = in_weight.shape
     groups, states, heads = b_real.shape
     lanes = groups * states
-    decay_re, decay_im, ratio_re, ratio_im = step_factors(lam_real, lam_imag, log_step)
-    factor = jnp.stack((decay_re.reshape(lanes), decay_im.reshape(lanes)), 0)
-    bbar_re = ratio_re[..., None] * b_real - ratio_im[..., None] * b_imag
-    bbar_im = ratio_re[..., None] * b_imag + ratio_im[..., None] * b_real
-    bmat = jnp.stack((bbar_re, bbar_im), 0).transpose(0, 3, 1, 2).reshape(2, heads, lanes)
-    cmat = jnp.stack((c_real, c_imag), 0).transpose(0, 2, 1, 3).reshape(2, heads, lanes)
     pieces = jnp.stack((lin_weight.T, gate_weight.T), 0)
     count = channels // LANES
     bf16, f32 = jnp.bfloat16, jnp.float32
@@ -391,12 +429,14 @@
     mixed = pl.pallas_call(
         functools.partial(kernel, sizes),
         out_shape=jax.ShapeDtypeStruct((tokens, width), bf16),
-        in_specs=[pl.BlockSpec(memory_space=pltpu.VMEM)] * 7,
+        in_specs=[pl.BlockSpec(memory_space=pltpu.VMEM)] * 11,
         out_specs=pl.BlockSpec(memory_space=pltpu.VMEM),
         scratch_shapes=[
             pltpu.VMEM((rows * sp * dp, channels), bf16),
             pltpu.VMEM((2, width, channels), bf16),
             pltpu.VMEM((8, count, LANES, lanes // count), bf16),
+            pltpu.VMEM((4, lanes), f32),
+            pltpu.VMEM((4, heads, lanes), f32),
             pltpu.VMEM((2, tokens, lanes), f32),
             pltpu.VMEM((2, SUBLANES, lanes), f32),
             pltpu.VMEM((2, SUBLANES, lanes), f32),
@@ -412,7 +452,19 @@
         compiler_params=pltpu.CompilerParams(
             collective_id=0, has_side_effects=True, vmem_limit_bytes=60 * 1024 * 1024
         ),
-    )(hidden_in[0], in_weight, pieces, factor, bmat, cmat, skip_weight[None])
+    )(
+        hidden_in[0],
+        in_weight,
+        pieces,
+        lam_real,
+        lam_imag,
+        log_step[:, None],
+        b_real.transpose(0, 2, 1),
+        b_imag.transpose(0, 2, 1),
+        c_real,
+        c_imag,
+        skip_weight[None],
+    )
     return mixed[None]
 
 

time: 54.4 us -> 51.3 us (0.943)
  other arithmetic: 3.41 us -> 1.54 us
  local copies, waits for them, and re-layouts: 4.81 us -> 3.22 us
    reshape x2 -> x0, local copies, waits for them, and re-layouts: 1.76 us -> none  [the longest x1 0.89 us: shards(): jnp.stack((bbar_re, bbar_im), 0).transpose(0, 3, 1, 2)]
    another operation x2 -> x0, other arithmetic: 1.72 us -> none  [the longest x1 1.1 us: shards(): jnp.stack((bbar_re, bbar_im), 0).transpose(0, 3, 1, 2)]
    div x1 -> x0, other arithmetic: 0.95 us -> none  [step_factors(): ratio_re = (numer_re * lam_real + decay_im * lam_imag) / magnitude]
    another operation x1, other arithmetic: 0.67 us -> 1.54 us  [shards(): pieces = jnp.stack((lin_weight.T, gate_weight.T), 0)]
    broadcast_in_dim x0 -> x1, local copies, waits for them, and re-layouts: none -> 0.69 us  [shards(): log_step[:, None]]
    exp x1 -> x0, local copies, waits for them, and re-layouts: 0.66 us -> none  [step_factors(): step = jnp.exp(log_step)[:, None]]
    unnamed x9 -> x3, local copies, waits for them, and re-layouts: 1.91 us -> 2.54 us
where the time goes in v2:
time: 51.3 us; the launch traced here: 50.7 us
  Pallas kernels  46 us (90%)
  local copies, waits for them, and re-layouts  3.22 us (6%)
  other arithmetic  1.54 us (3%)
    pallas_call x1, Pallas kernels, shards(): pl.pallas_call(functools.partial(kernel, sizes), out_shape=jax.ShapeDtype...  46 us
    unnamed x3, local copies, waits for them, and re-layouts  2.54 us
    another operation x1, other arithmetic, shards(): pieces = jnp.stack((lin_weight.T, gate_weight.T), 0)  1.54 us

profile of v2, /device:TPU:0, one launch (start us, length us, event | category | flops | bytes accessed | tf_op | source)
XLA Modules:
  0.0 50.7 jit_solution(17884419356516484419)
XLA Ops:
  0.0 0.0 copy-start
  0.0 0.7 %copy-done = f32[32]{0:T(128)S(1)} copy-done((f32[32]{0:T(128)S(1)}, f32[32]{0:T(128)}, u32[]{:S(2)}) %copy-start) | copy-done | bytes 152
  0.7 0.7 %copy.13.log_step_ref = f32[32,1]{1,0:T(8,128)} copy(f32[32,1]{0,1:T(1,128)S(1)} %bitcast.19) | data formatting | bytes 256 | tf_op jit(solution)/shard_map/broadcast_in_dim | solution.py:461
  1.3 1.5 %pad_maximum_fusion.wout_ref = bf16[2,64,512]{2,1,0:T(8,128)(2,1)} fusion(bf16[1,64,512]{2,1,0:T(8,128)(2,1)} %bitcast.16, bf16[1,64,512]{2,1,0:T(8,128)(2,1)} %bitcast.17), kind=kLoop, calls=%fused_computation | loop fusion | flops 65536 | bytes 262144 | tf_op jit(solution)/shard_map/stack | solution.py:425
  2.9 46.0 %shard_map.118 = bf16[128,2048]{1,0:T(8,128)(2,1)} custom-call(bf16[128,2048]{1,0:T(8,128)(2,1)} %bitcast.13, bf16[64,512]{1,0:T(8,128)(2,1)} %win_ref.1, bf16[2,64,512]{2,1,0:T(8,128)(2,1)} %pad_maximum_fusion.wout_ref, f32[32,64]{1,0:T(8,128)} %lam_re_ref.1, f32[32,64]{1,0:T(8,128)} %lam_im_ref.1, f32[32,1]{1,0:T(8,128)} %copy.13.log_step_ref, ...), custom_call_target="tpu_custom_call" | custom-call | tf_op jit(solution)/shard_map/pallas_call | solution.py:429
  48.9 1.9 %copy.15 = bf16[1,128,2048]{2,1,0:T(8,128)(2,1)} copy(bf16[1,128,2048]{2,1,0:T(8,128)(2,1)} %bitcast.12) | data formatting | bytes 1048576
Async XLA Ops:
  0.0 0.7 %copy-start = (f32[32]{0:T(128)S(1)}, f32[32]{0:T(128)}, u32[]{:S(2)}) copy-start(f32[32]{0:T(128)} %param.16) | copy-start | bytes 388
